TPU v7x, 32 devices: a whole 2x2x4 slice. The times are simulated.
32 devices in a mesh: sp: 8 (over z, y), tp: 4 (over x, core).
Axes of the slice: x: 2, y: 2, z: 4, core: 2. Of those that a mesh axis runs over, the one named last changes fastest.
Arguments:
- query_rows: bfloat16 [4096, 1024], P('sp', 'tp'), may hold values from -6 to 6
- key_rows: bfloat16 [4096, 512], P('sp', 'tp'), may hold values from -6 to 6
- value_rows: bfloat16 [4096, 512], P('sp', 'tp'), may hold values from -12 to 12
- query_gain: float32 [128], replicated, may hold values from 0.2 to 6.5
- key_gain: float32 [128], replicated, may hold values from 0.2 to 6.5
- residual: bfloat16 [4096, 2048], P(('sp', 'tp')), may hold values from -6 to 6
- out_weight: bfloat16 [1024, 2048], P('tp'), may hold values from -3 to 3
- mix_gain: float32 [2048], replicated, may hold values from 0.1 to 1.9
- gate_weight: bfloat16 [2048, 5632], P('sp', 'tp'), may hold values from -0.125 to 0.125
- up_weight: bfloat16 [2048, 5632], P('sp', 'tp'), may hold values from -0.125 to 0.125
- down_weight: bfloat16 [5632, 2048], P('tp', 'sp'), may hold values from -0.15625 to 0.15625
Outputs:
- layer_out: bfloat16 [4096, 2048], P(('sp', 'tp'))
All inputs are finite; a program needn't handle non-finite values.
Results may differ from a plain program's by a relative error of at most 0.015.
The roundings to bfloat16 on the way count: a program that leaves them out, or rounds other values in their place, can miss the bound.
Values may be sent and summed in bfloat16 or wider, within the bound.
A program may use at most 128 MiB of HBM per device.

v0:
```python
import jax
import jax.numpy as jnp
from jax import lax
from jax.sharding import PartitionSpec as P

GRID = 64
norm_eps = 1e-06
theta_base = 10000.0


def spin(halfway, angles):
    cosine = jnp.cos(angles)[:, None, :]
    sine_val = jnp.sin(angles)[:, None, :]
    quarter = halfway.shape[-1] // 2
    leading = halfway[..., :quarter]
    trailing = halfway[..., quarter:]
    return [leading * cosine - trailing * sine_val, trailing * cosine + leading * sine_val]


def rotate_grid(vectors, positions):
    head_dim = vectors.shape[-1]
    quarter = head_dim // 4
    frequency = jnp.power(
        theta_base, -2.0 * jnp.arange(quarter, dtype=jnp.float32) / (head_dim // 2)
    )
    row_angle = (positions // GRID).astype(jnp.float32)[:, None] * frequency
    col_angle = (positions % GRID).astype(jnp.float32)[:, None] * frequency
    lower_half = vectors[..., : 2 * quarter]
    upper_half = vectors[..., 2 * quarter :]
    return jnp.concatenate(spin(lower_half, row_angle) + spin(upper_half, col_angle), axis=-1)


def prepare_heads(raw_heads, head_gain, positions):
    floated = raw_heads.astype(jnp.float32)
    scaled = floated * lax.rsqrt(jnp.mean(floated * floated, axis=-1, keepdims=True) + norm_eps)
    return rotate_grid(scaled * head_gain, positions).astype(jnp.bfloat16)


def row_norm(row_data, row_gain):
    floated = row_data.astype(jnp.float32)
    scaled = floated * lax.rsqrt(jnp.mean(floated * floated, axis=-1, keepdims=True) + norm_eps)
    return (scaled * row_gain).astype(jnp.bfloat16)


def on_device(
    query_rows,
    key_rows,
    value_rows,
    query_gain,
    key_gain,
    residual,
    out_weight,
    mix_gain,
    gate_weight,
    up_weight,
    down_weight,
):
    tok_rows = query_rows.shape[0]
    head_dim = query_gain.shape[0]
    local_kv = key_rows.shape[1] // head_dim
    local_q = query_rows.shape[1] // head_dim
    group_size = local_q // local_kv
    positions = lax.axis_index("sp") * tok_rows + jnp.arange(tok_rows, dtype=jnp.int32)
    gate_whole, up_whole, down_whole = (
        lax.all_gather(gate_weight, "sp", axis=0, tiled=True),
        lax.all_gather(up_weight, "sp", axis=0, tiled=True),
        lax.all_gather(down_weight, "sp", axis=1, tiled=True),
    )
    q_heads = prepare_heads(query_rows.reshape(tok_rows, local_q, head_dim), query_gain, positions)
    q_stack = (
        q_heads.reshape(tok_rows, local_kv, group_size, head_dim)
        .transpose(1, 2, 0, 3)
        .reshape(local_kv, group_size * tok_rows, head_dim)
    )
    k_heads = prepare_heads(
        key_rows.reshape(tok_rows, local_kv, head_dim), key_gain, positions
    ).reshape(tok_rows, local_kv * head_dim)
    score_scale = head_dim ** (-0.5)
    start_state = (
        jnp.full((local_kv, group_size * tok_rows), -jnp.inf, jnp.float32),
        jnp.zeros((local_kv, group_size * tok_rows), jnp.float32),
        jnp.zeros((local_kv, group_size * tok_rows, head_dim), jnp.float32),
    )
    key_piece = lax.all_gather(k_heads, "sp", axis=0, tiled=True)
    value_piece = lax.all_gather(value_rows, "sp", axis=0, tiled=True)
    count_rows = key_piece.shape[0]
    key_blocks = key_piece.reshape(count_rows // tok_rows, tok_rows, local_kv, head_dim).transpose(
        0, 2, 1, 3
    )
    value_blocks = value_piece.reshape(
        count_rows // tok_rows, tok_rows, local_kv, head_dim
    ).transpose(0, 2, 1, 3)

    def inner(state, blocks):
        key_block, value_block = blocks
        running_max, running_sum, weighted = state
        scores = (
            jnp.einsum("kqd,ksd->kqs", q_stack, key_block, preferred_element_type=jnp.float32)
            * score_scale
        )
        new_max = jnp.maximum(running_max, jnp.max(scores, axis=-1))
        weights = jnp.exp(scores - new_max[..., None])
        factor = jnp.exp(running_max - new_max)
        running_sum = running_sum * factor + jnp.sum(weights, axis=-1)
        weighted = weighted * factor[..., None] + jnp.einsum(
            "kqs,ksd->kqd",
            weights.astype(jnp.bfloat16),
            value_block,
            preferred_element_type=jnp.float32,
        )
        return ((new_max, running_sum, weighted), None)

    result, unused = lax.scan(inner, start_state, (key_blocks, value_blocks))
    final_max, final_sum, weighted = result
    attended = (weighted / final_sum[..., None]).reshape(local_kv, group_size, tok_rows, head_dim)
    attended = (
        attended.transpose(2, 0, 1, 3).reshape(tok_rows, local_q * head_dim).astype(jnp.bfloat16)
    )
    attn_sum = lax.psum_scatter(
        jnp.dot(attended, out_weight, preferred_element_type=jnp.float32).astype(jnp.bfloat16),
        "tp",
        scatter_dimension=0,
        tiled=True,
    ).astype(jnp.float32)
    own_rows = (residual.astype(jnp.float32) + attn_sum).astype(jnp.bfloat16)
    normed_all = lax.all_gather(row_norm(own_rows, mix_gain), "tp", axis=0, tiled=True)
    gate_act = jnp.dot(normed_all, gate_whole, preferred_element_type=jnp.float32)
    up_act = jnp.dot(normed_all, up_whole, preferred_element_type=jnp.float32)
    hidden = (jax.nn.silu(gate_act) * up_act).astype(jnp.bfloat16)
    unit_sum = lax.psum_scatter(
        jnp.dot(hidden, down_whole, preferred_element_type=jnp.float32).astype(jnp.bfloat16),
        "tp",
        scatter_dimension=0,
        tiled=True,
    ).astype(jnp.float32)
    return (own_rows.astype(jnp.float32) + 0.5 * unit_sum).astype(jnp.bfloat16)


def solution(mesh):
    placed = (
        P("sp", "tp"),
        P("sp", "tp"),
        P("sp", "tp"),
        P(),
        P(),
        P(("sp", "tp"), None),
        P("tp", None),
        P(),
        P("sp", "tp"),
        P("sp", "tp"),
        P("tp", "sp"),
    )
    return jax.shard_map(
        on_device, mesh=mesh, in_specs=placed, out_specs=P(("sp", "tp"), None), check_vma=False
    )
```

profile of v0, /device:TPU:0, one launch (start us, length us, event | category | flops | bytes accessed | tf_op | source)
XLA Modules:
  0.0 523.7 jit_solution(12080952115448605212)
XLA Ops:
  12.5 1.9 multiply_cosine_fusion.1
  15.1 1.8 fusion.26
  16.9 1.6 maximum_bitcast_fusion
  18.5 33.5 %all-gather.7.cloned.1.call-done = bf16[4096,128]{0,1:T(8,128)(2,1)} async-done(((bf16[512,128]{0,1:T(8,128)(2,1)}), bf16[4096,128]{0,1:T(8,128)(2,1)}) %all-gather.7.cloned.1.call-update) | async-done | bytes 1048592 | tf_op jit(solution)/shard_map/all_gather | solution.py:84
  52.0 2.3 copy.24
  54.3 39.2 %all-gather.9.cloned.1.call-done = bf16[4096,128]{1,0:T(8,128)(2,1)} async-done(((bf16[512,128]{1,0:T(8,128)(2,1)}), bf16[4096,128]{1,0:T(8,128)(2,1)}) %all-gather.9.cloned.1.call-update) | async-done | bytes 1048592 | tf_op jit(solution)/shard_map/all_gather | solution.py:85
  93.5 37.9 %while.15 = (s32[]{:T(128)}, f32[1,1024]{1,0:T(1,128)S(1)}, f32[1,1024]{1,0:T(1,128)S(1)}, f32[1,1024,128]{2,1,0:T(8,128)}, bf16[8,1,512,128]{3,2,1,0:T(8,128)(2...) while((s32[]{:T(128)}, f32[1,1024]{1,0:T(1,128)S(1)}, ...), condition=%wide.region_5.6_spmd.clone, body=%wide.region_2.5_spmd.clone.sunk | while | flops 273028096 | bytes 12125345 | solution.py:113
  95.9 1.5 fusion.75
  98.2 1.3 multiply_reduce_fusion.3
  100.6 1.5 fusion.75
  102.9 1.3 multiply_reduce_fusion.3
  105.3 1.5 fusion.75
  107.7 1.3 multiply_reduce_fusion.3
  110.1 1.5 fusion.75
  112.4 1.3 multiply_reduce_fusion.3
  114.8 1.5 fusion.75
  117.1 1.3 multiply_reduce_fusion.3
  119.5 1.5 fusion.75
  124.3 1.5 fusion.75
  126.6 1.3 multiply_reduce_fusion.3
  129.0 1.5 fusion.75
  132.8 2.1 convolution_convert_fusion
  134.9 30.0 %reduce-scatter.3.cloned.1.call-done = bf16[128,2048]{1,0:T(8,128)(2,1)} async-done(((bf16[512,2048]{1,0:T(8,128)(2,1)}), bf16[128,2048]{1,0:T(8,128)(2,1)}) %reduce-scatter.3.cloned.1.call-update) | async-done | bytes 524304 | tf_op jit(solution)/shard_map/reduce_scatter | solution.py:119
  166.2 2.0 fusion.21
  170.4 20.6 %all-gather.11.cloned.1.call-done = bf16[512,2048]{1,0:T(8,128)(2,1)} async-done(((bf16[128,2048]{1,0:T(8,128)(2,1)}), bf16[512,2048]{1,0:T(8,128)(2,1)}) %all-gather.11.cloned.1.call-update) | async-done | bytes 2097168 | tf_op jit(solution)/shard_map/all_gather | solution.py:126
  191.0 94.4 %all-gather.13.cloned.1.call-done = bf16[2048,1408]{1,0:T(8,128)(2,1)} async-done(((bf16[256,1408]{1,0:T(8,128)(2,1)}), bf16[2048,1408]{1,0:T(8,128)(2,1)}) %all-gather.13.cloned.1.call-update) | async-done | bytes 5767184 | tf_op jit(solution)/shard_map/all_gather | solution.py:65
  285.4 8.2 %fusion.56 = f32[512,1408]{1,0:T(8,128)} fusion(bf16[512,2048]{1,0:T(8,128)(2,1)} %all-gather.11.cloned.1.call-done, bf16[2048,1408]{1,0:T(8,128)(2,1)} %all-gather.13.cloned.1.call-done), kind=kOutput, calls=%fused_computation.99 | convolution fusion | flops 2952790016 | bytes 10747904 | tf_op jit(solution)/shard_map/dot_general | solution.py:127
  293.6 84.3 %all-gather.15.cloned.1.call-done = bf16[2048,1408]{1,0:T(8,128)(2,1)} async-done(((bf16[256,1408]{1,0:T(8,128)(2,1)}), bf16[2048,1408]{1,0:T(8,128)(2,1)}) %all-gather.15.cloned.1.call-update) | async-done | bytes 5767184 | tf_op jit(solution)/shard_map/all_gather | solution.py:66
  377.9 93.4 %all-gather.17.cloned.1.call-done = bf16[1408,2048]{1,0:T(8,128)(2,1)} async-done(((bf16[1408,256]{1,0:T(8,128)(2,1)}), bf16[1408,2048]{1,0:T(8,128)(2,1)}) %all-gather.17.cloned.1.call-update) | async-done | bytes 5767184 | tf_op jit(solution)/shard_map/all_gather | solution.py:67
  471.3 14.0 %convolution_convert_fusion.1 = bf16[512,2048]{1,0:T(8,128)(2,1)} fusion(bf16[1408,2048]{1,0:T(8,128)(2,1)} %all-gather.17.cloned.1.call-done, bf16[512,2048]{1,0:T(8,128)(2,1)} %all-gather.11.cloned.1.call-done, bf16[2048,1408]{1,0:T(8,128)(2,1)} %all-gather.15.cloned.1.call-done, f32[512,1408]{1,0:T(8,128)} %fusion.56), kind=kOutput, calls=%fused_computation.27 | convolution fusion | flops 5910953984 | bytes 18612224 | tf_op jit(solution)/shard_map/dot_general | solution.py:131
  485.3 29.5 %reduce-scatter.5.cloned.1.call-done = bf16[128,2048]{1,0:T(8,128)(2,1)} async-done(((bf16[512,2048]{1,0:T(8,128)(2,1)}), bf16[128,2048]{1,0:T(8,128)(2,1)}) %reduce-scatter.5.cloned.1.call-update) | async-done | bytes 524304 | tf_op jit(solution)/shard_map/reduce_scatter | solution.py:130
  514.8 2.1 fusion.22
  (112 shorter events, 28.6 us)
Async XLA Ops:
  6.5 126.2 %copy-start = (bf16[256,2048]{1,0:T(8,128)(2,1)S(1)}, bf16[256,2048]{1,0:T(8,128)(2,1)}, u32[]{:S(2)}) copy-start(bf16[256,2048]{1,0:T(8,128)(2,1)} %param.19) | copy-start | bytes 3145732
  6.5 45.5 %all-gather.7.cloned.1.call-start = ((), (), s32[]{:S(2)}) async-start(), calls=%async_computation.2 | async-start | bytes 1179648 | tf_op jit(solution)/shard_map/all_gather | solution.py:84
  8.5 5.9 %copy-start.6 = (f32[128]{0:T(128)S(1)}, f32[128]{0:T(128)}, u32[]{:S(2)}) copy-start(f32[128]{0:T(128)} %param.16) | copy-start | bytes 1540
  9.7 83.7 %all-gather.9.cloned.1.call-start = ((), (), s32[]{:S(2)}) async-start(), calls=%async_computation.3 | async-start | bytes 1179648 | tf_op jit(solution)/shard_map/all_gather | solution.py:85
  10.5 154.4 %reduce-scatter.3.cloned.1.call-start = ((), (), s32[]{:S(2)}) async-start(), calls=%async_computation.4 | async-start | bytes 2621440 | tf_op jit(solution)/shard_map/reduce_scatter | solution.py:119
  94.8 1.0 copy-start.1
  97.4 0.8 copy-start.2
  99.6 1.0 copy-start.1
  102.2 0.8 copy-start.2
  104.3 1.0 copy-start.1
  106.9 0.8 copy-start.2
  109.0 1.0 copy-start.1
  111.6 0.8 copy-start.2
  113.8 1.0 copy-start.1
  116.3 0.8 copy-start.2
  118.5 1.0 copy-start.1
  121.1 0.8 copy-start.2
  123.2 1.0 copy-start.1
  125.8 0.8 copy-start.2
  128.0 1.0 copy-start.1
  130.5 0.8 copy-start.2
  134.8 30.0 %copy-start.3 = (bf16[128,2048]{1,0:T(8,128)(2,1)S(1)}, bf16[128,2048]{1,0:T(8,128)(2,1)}, u32[]{:S(2)}) copy-start(bf16[128,2048]{1,0:T(8,128)(2,1)} %param.18) | copy-start | bytes 1572868
  134.8 31.4 %copy-start.5 = (f32[2048]{0:T(1024)S(1)}, f32[2048]{0:T(1024)}, u32[]{:S(2)}) copy-start(f32[2048]{0:T(1024)} %param.20) | copy-start | bytes 24580
  134.9 56.1 %all-gather.11.cloned.1.call-start = ((), (), s32[]{:S(2)}) async-start(), calls=%async_computation.5 | async-start | bytes 2621440 | tf_op jit(solution)/shard_map/all_gather | solution.py:126
  168.3 117.1 %all-gather.13.cloned.1.call-start = ((), (), s32[]{:S(2)}) async-start(), calls=%async_computation.6 | async-start | bytes 6488064 | tf_op jit(solution)/shard_map/all_gather | solution.py:65
  168.9 209.1 %all-gather.15.cloned.1.call-start = ((), (), s32[]{:S(2)}) async-start(), calls=%async_computation.7 | async-start | bytes 6488064 | tf_op jit(solution)/shard_map/all_gather | solution.py:66
  169.4 301.9 %all-gather.17.cloned.1.call-start = ((), (), s32[]{:S(2)}) async-start(), calls=%async_computation.8 | async-start | bytes 6488064 | tf_op jit(solution)/shard_map/all_gather | solution.py:67
  170.2 344.6 %reduce-scatter.5.cloned.1.call-start = ((), (), s32[]{:S(2)}) async-start(), calls=%async_computation.9 | async-start | bytes 2621440 | tf_op jit(solution)/shard_map/reduce_scatter | solution.py:130
  485.3 29.5 %copy-start.4 = (bf16[128,2048]{1,0:T(8,128)(2,1)S(1)}, bf16[128,2048]{1,0:T(8,128)(2,1)}, u32[]{:S(2)}) copy-start(bf16[128,2048]{1,0:T(8,128)(2,1)} %reduce-scatter.3.cloned.1.call-done) | copy-start | bytes 1572868
Sparse Core Ops, SparseCore 0:
  9.9 42.1 all-gather.6
  54.2 39.2 all-gather.8
  135.0 29.8 reduce-scatter.2
  168.4 22.5 all-gather.10
  193.0 92.3 all-gather.12
  287.4 90.4 all-gather.14
  380.0 91.2 all-gather.16
  485.4 29.3 reduce-scatter.4
where the time goes:
time: 525 us; the launch traced here: 524 us
  waiting for transfers between devices  427 us (81%)
  matrix products  47.2 us (9%)
  other arithmetic  18.6 us (4%)
  local copies, waits for them, and re-layouts  16.1 us (3%)
  between operations  13.6 us (3%)
    all_gather x1, waiting for transfers between devices, on_device(): lax.all_gather(gate_weight, 'sp', axis=0, tiled=True)  94.4 us
    all_gather x1, waiting for transfers between devices, on_device(): lax.all_gather(down_weight, 'sp', axis=1, tiled=True)  93.4 us
    all_gather x1, waiting for transfers between devices, on_device(): lax.all_gather(up_weight, 'sp', axis=0, tiled=True)  84.3 us
    all_gather x1, waiting for transfers between devices, on_device(): value_piece = lax.all_gather(value_rows, 'sp', axis=0, tiled=True)  39.2 us
    all_gather x1, waiting for transfers between devices, on_device(): key_piece = lax.all_gather(k_heads, 'sp', axis=0, tiled=True)  33.5 us
    reduce_scatter x1, waiting for transfers between devices, on_device(): lax.psum_scatter(jnp.dot(attended, out_weight, preferred_element_type=jnp...  30 us
    reduce_scatter x1, waiting for transfers between devices, on_device(): lax.psum_scatter(jnp.dot(hidden, down_whole, preferred_element_type=jnp.f...  29.5 us
    all_gather x1, waiting for transfers between devices, on_device(): lax.all_gather(row_norm(own_rows, mix_gain), 'tp', axis=0, tiled=True)  20.6 us
  transfers between devices with their start and end apart: 8, of which 8 were waited for; matrix products, arithmetic and copies ran while one was open for 4% of the time, Pallas kernels for 0%

commit v1 on v0

--- a/solution.py
+++ b/solution.py
@@ -2,6 +2,7 @@
 import jax.numpy as jnp
 from jax import lax
 from jax.sharding import PartitionSpec as P
+from jax.lax import axis_index, axis_size, ppermute
 
 GRID = 64
 norm_eps = 1e-06
@@ -55,6 +56,20 @@
     up_weight,
     down_weight,
 ):
+
+    def create_pairs_all(m):
+        n_chips = axis_size("sp")
+        sheets = []
+        for u in range(n_chips):
+            sheets.append((u, (u + 1) % n_chips))
+        mat_out = [None] * n_chips
+        mat_out[n_chips - 1] = m
+        for dd in range(n_chips - 2, -1, -1):
+            mat_out[dd] = ppermute(mat_out[dd + 1], "sp", sheets)
+        passed = jnp.concatenate(mat_out, axis=0)
+        out_arr = (axis_index("sp") + 1) * m.shape[0]
+        return jnp.roll(passed, out_arr, axis=0)
+
     tok_rows = query_rows.shape[0]
     head_dim = query_gain.shape[0]
     local_kv = key_rows.shape[1] // head_dim
@@ -82,7 +97,7 @@
         jnp.zeros((local_kv, group_size * tok_rows, head_dim), jnp.float32),
     )
     key_piece = lax.all_gather(k_heads, "sp", axis=0, tiled=True)
-    value_piece = lax.all_gather(value_rows, "sp", axis=0, tiled=True)
+    value_piece = create_pairs_all(value_rows)
     count_rows = key_piece.shape[0]
     key_blocks = key_piece.reshape(count_rows // tok_rows, tok_rows, local_kv, head_dim).transpose(
         0, 2, 1, 3

time: 525 us -> 498 us (0.949)
  waiting for transfers between devices: 427 us -> 396 us
    ppermute x0 -> x7, waiting for transfers between devices: none -> 43.9 us  [create_pairs_all(): mat_out[dd] = ppermute(mat_out[dd + 1], 'sp', sheets)]
    all_gather x1 -> x0, waiting for transfers between devices: 39.2 us -> none  [on_device(): value_piece = lax.all_gather(value_rows, 'sp', axis=0, tiled=True)]
    all_gather x1, waiting for transfers between devices: 33.5 us -> 0.01 us  [on_device(): key_piece = lax.all_gather(k_heads, 'sp', axis=0, tiled=True)]
  transfers between devices with their start and end apart: 8 -> 14, of which waited for: 8 -> 13; matrix products, arithmetic and copies ran while one was open for 4% -> 4% of each run, Pallas kernels for 0% -> 0%
where the time goes in v1:
time: 498 us; the launch traced here: 497 us
  waiting for transfers between devices  396 us (80%)
  matrix products  47.2 us (9%)
  other arithmetic  18.6 us (4%)
  local copies, waits for them, and re-layouts  17.4 us (3%)
  between operations  13.8 us (3%)
    all_gather x1, waiting for transfers between devices, on_device(): lax.all_gather(gate_weight, 'sp', axis=0, tiled=True)  94.4 us
    all_gather x1, waiting for transfers between devices, on_device(): lax.all_gather(down_weight, 'sp', axis=1, tiled=True)  93.2 us
    all_gather x1, waiting for transfers between devices, on_device(): lax.all_gather(up_weight, 'sp', axis=0, tiled=True)  84.3 us
    ppermute x7, waiting for transfers between devices, create_pairs_all(): mat_out[dd] = ppermute(mat_out[dd + 1], 'sp', sheets)  43.9 us
    reduce_scatter x1, waiting for transfers between devices, on_device(): lax.psum_scatter(jnp.dot(hidden, down_whole, preferred_element_type=jnp.f...  29.5 us
    reduce_scatter x1, waiting for transfers between devices, on_device(): lax.psum_scatter(jnp.dot(attended, out_weight, preferred_element_type=jnp...  28.6 us
    all_gather x1, waiting for transfers between devices, on_device(): lax.all_gather(row_norm(own_rows, mix_gain), 'tp', axis=0, tiled=True)  20.7 us
    dot_general x1, matrix products, on_device(): jnp.dot(hidden, down_whole, preferred_element_type=jnp.float32)  13.9 us
  transfers between devices with their start and end apart: 14, of which 13 were waited for; matrix products, arithmetic and copies ran while one was open for 4% of the time, Pallas kernels for 0%

profile of v1, /device:TPU:0, one launch (start us, length us, event | category | flops | bytes accessed | tf_op | source)
XLA Modules:
  0.0 497.1 jit_solution(14962767185020572494)
XLA Ops:
  6.5 3.0 collective-permute-start
  11.4 4.9 collective-permute-done
  18.8 5.1 %collective-permute-done.1 = bf16[512,128]{1,0:T(8,128)(2,1)S(1)} collective-permute-done((bf16[512,128]{1,0:T(8,128)(2,1)S(1)}, bf16[512,128]{1,0:T(8,128)(2,1)S(1)}, u32[]{:S(2)}, u32[]{:S(2)}) %collective-permute-start.1) | collective-permute-done | bytes 131104 | tf_op jit(solution)/shard_map/ppermute | solution.py:68
  24.6 7.1 %collective-permute-done.2 = bf16[512,128]{1,0:T(8,128)(2,1)S(1)} collective-permute-done((bf16[512,128]{1,0:T(8,128)(2,1)S(1)}, bf16[512,128]{1,0:T(8,128)(2,1)S(1)}, u32[]{:S(2)}, u32[]{:S(2)}) %collective-permute-start.2) | collective-permute-done | bytes 131104 | tf_op jit(solution)/shard_map/ppermute | solution.py:68
  31.8 8.0 %collective-permute-done.3 = bf16[512,128]{1,0:T(8,128)(2,1)S(1)} collective-permute-done((bf16[512,128]{1,0:T(8,128)(2,1)S(1)}, bf16[512,128]{1,0:T(8,128)(2,1)S(1)}, u32[]{:S(2)}, u32[]{:S(2)}) %collective-permute-start.3) | collective-permute-done | bytes 131104 | tf_op jit(solution)/shard_map/ppermute | solution.py:68
  40.5 7.0 %collective-permute-done.4 = bf16[512,128]{1,0:T(8,128)(2,1)S(1)} collective-permute-done((bf16[512,128]{1,0:T(8,128)(2,1)S(1)}, bf16[512,128]{1,0:T(8,128)(2,1)S(1)}, u32[]{:S(2)}, u32[]{:S(2)}) %collective-permute-start.4) | collective-permute-done | bytes 131104 | tf_op jit(solution)/shard_map/ppermute | solution.py:68
  47.5 1.9 multiply_cosine_fusion.1
  49.4 7.6 %collective-permute-done.5 = bf16[512,128]{1,0:T(8,128)(2,1)S(1)} collective-permute-done((bf16[512,128]{1,0:T(8,128)(2,1)S(1)}, bf16[512,128]{1,0:T(8,128)(2,1)S(1)}, u32[]{:S(2)}, u32[]{:S(2)}) %collective-permute-start.5) | collective-permute-done | bytes 131104 | tf_op jit(solution)/shard_map/ppermute | solution.py:68
  57.0 1.8 fusion.26
  58.8 1.6 maximum_bitcast_fusion
  60.5 4.1 collective-permute-done.6
  66.1 2.3 copy.24
  68.4 37.9 %while.15 = (s32[]{:T(128)}, f32[1,1024]{1,0:T(1,128)S(1)}, f32[1,1024]{1,0:T(1,128)S(1)}, f32[1,1024,128]{2,1,0:T(8,128)}, bf16[8,1,512,128]{3,2,1,0:T(8,128)(2...) while((s32[]{:T(128)}, f32[1,1024]{1,0:T(1,128)S(1)}, ...), condition=%wide.region_5.6_spmd.clone, body=%wide.region_2.5_spmd.clone.sunk | while | flops 273028096 | bytes 12125345 | solution.py:128
  70.8 1.5 fusion.75
  75.5 1.5 fusion.75
  80.3 1.5 fusion.75
  85.0 1.5 fusion.75
  89.7 1.5 fusion.75
  94.5 1.5 fusion.75
  99.2 1.5 fusion.75
  103.9 1.5 fusion.75
  107.7 2.1 convolution_convert_fusion
  109.8 28.6 %reduce-scatter.3.cloned.1.call-done = bf16[128,2048]{1,0:T(8,128)(2,1)} async-done(((bf16[512,2048]{1,0:T(8,128)(2,1)}), bf16[128,2048]{1,0:T(8,128)(2,1)}) %reduce-scatter.3.cloned.1.call-update) | async-done | bytes 524304 | tf_op jit(solution)/shard_map/reduce_scatter | solution.py:134
  139.8 2.0 fusion.21
  143.8 20.7 %all-gather.8.cloned.1.call-done = bf16[512,2048]{1,0:T(8,128)(2,1)} async-done(((bf16[128,2048]{1,0:T(8,128)(2,1)}), bf16[512,2048]{1,0:T(8,128)(2,1)}) %all-gather.8.cloned.1.call-update) | async-done | bytes 2097168 | tf_op jit(solution)/shard_map/all_gather | solution.py:141
  164.5 94.4 %all-gather.10.cloned.1.call-done = bf16[2048,1408]{1,0:T(8,128)(2,1)} async-done(((bf16[256,1408]{1,0:T(8,128)(2,1)}), bf16[2048,1408]{1,0:T(8,128)(2,1)}) %all-gather.10.cloned.1.call-update) | async-done | bytes 5767184 | tf_op jit(solution)/shard_map/all_gather | solution.py:80
  258.9 8.2 %fusion.56 = f32[512,1408]{1,0:T(8,128)} fusion(bf16[512,2048]{1,0:T(8,128)(2,1)} %all-gather.8.cloned.1.call-done, bf16[2048,1408]{1,0:T(8,128)(2,1)} %all-gather.10.cloned.1.call-done), kind=kOutput, calls=%fused_computation.116 | convolution fusion | flops 2952790016 | bytes 10747904 | tf_op jit(solution)/shard_map/dot_general | solution.py:142
  267.2 84.3 %all-gather.12.cloned.1.call-done = bf16[2048,1408]{1,0:T(8,128)(2,1)} async-done(((bf16[256,1408]{1,0:T(8,128)(2,1)}), bf16[2048,1408]{1,0:T(8,128)(2,1)}) %all-gather.12.cloned.1.call-update) | async-done | bytes 5767184 | tf_op jit(solution)/shard_map/all_gather | solution.py:81
  351.5 93.2 %all-gather.14.cloned.1.call-done = bf16[1408,2048]{1,0:T(8,128)(2,1)} async-done(((bf16[1408,256]{1,0:T(8,128)(2,1)}), bf16[1408,2048]{1,0:T(8,128)(2,1)}) %all-gather.14.cloned.1.call-update) | async-done | bytes 5767184 | tf_op jit(solution)/shard_map/all_gather | solution.py:82
  444.7 13.9 %convolution_convert_fusion.1 = bf16[512,2048]{1,0:T(8,128)(2,1)} fusion(bf16[1408,2048]{1,0:T(8,128)(2,1)} %all-gather.14.cloned.1.call-done, bf16[512,2048]{1,0:T(8,128)(2,1)} %all-gather.8.cloned.1.call-done, bf16[2048,1408]{1,0:T(8,128)(2,1)} %all-gather.12.cloned.1.call-done, f32[512,1408]{1,0:T(8,128)} %fusion.56), kind=kOutput, calls=%fused_computation.27 | convolution fusion | flops 5910953984 | bytes 18612224 | tf_op jit(solution)/shard_map/dot_general | solution.py:146
  458.7 29.5 %reduce-scatter.5.cloned.1.call-done = bf16[128,2048]{1,0:T(8,128)(2,1)} async-done(((bf16[512,2048]{1,0:T(8,128)(2,1)}), bf16[128,2048]{1,0:T(8,128)(2,1)}) %reduce-scatter.5.cloned.1.call-update) | async-done | bytes 524304 | tf_op jit(solution)/shard_map/reduce_scatter | solution.py:145
  488.2 2.1 fusion.22
  (142 shorter events, 37.1 us)
Async XLA Ops:
  6.5 101.1 %copy-start = (bf16[256,2048]{1,0:T(8,128)(2,1)S(1)}, bf16[256,2048]{1,0:T(8,128)(2,1)}, u32[]{:S(2)}) copy-start(bf16[256,2048]{1,0:T(8,128)(2,1)} %param.19) | copy-start | bytes 3145732
  6.5 33.3 %copy-start.7 = (f32[128]{0:T(128)S(1)}, f32[128]{0:T(128)}, u32[]{:S(2)}) copy-start(f32[128]{0:T(128)} %param.16) | copy-start | bytes 1540
  6.5 59.6 %all-gather.6.cloned.1.call-start = ((), (), s32[]{:S(2)}) async-start(), calls=%async_computation.2 | async-start | bytes 1179648 | tf_op jit(solution)/shard_map/all_gather | solution.py:99
  6.5 9.7 %collective-permute-start = (bf16[512,128]{1,0:T(8,128)(2,1)}, bf16[512,128]{1,0:T(8,128)(2,1)S(1)}, u32[]{:S(2)}, u32[]{:S(2)}) collective-permute-start(bf16[512,128]{1,0:T(8,128)(2,1)} %param.15), channel_id=1, source_target_pairs={{0,4},{4,8},{8,12},{12,16},{16,20},{20,24},{24,28},{28,0},{1,5},{5... | collective-permute-start | bytes 393224 | tf_op jit(solution)/shard_map/ppermute | solution.py:68
  16.3 7.7 %collective-permute-start.1 = (bf16[512,128]{1,0:T(8,128)(2,1)S(1)}, bf16[512,128]{1,0:T(8,128)(2,1)S(1)}, u32[]{:S(2)}, u32[]{:S(2)}) collective-permute-start(bf16[512,128]{1,0:T(8,128)(2,1)S(1)} %collective-permute-done), channel_id=1, source_target_pairs={{0,4},{4,8},{8,12},{12,16},{16,20},{20,24},{24,28},{28,0},{1,5},{5... | collective-permute-start | bytes 393224 | tf_op jit(solution)/shard_map/ppermute | solution.py:68
  17.5 120.9 %reduce-scatter.3.cloned.1.call-start = ((), (), s32[]{:S(2)}) async-start(), calls=%async_computation.3 | async-start | bytes 2621440 | tf_op jit(solution)/shard_map/reduce_scatter | solution.py:134
  23.9 7.8 %collective-permute-start.2 = (bf16[512,128]{1,0:T(8,128)(2,1)S(1)}, bf16[512,128]{1,0:T(8,128)(2,1)S(1)}, u32[]{:S(2)}, u32[]{:S(2)}) collective-permute-start(bf16[512,128]{1,0:T(8,128)(2,1)S(1)} %collective-permute-done.1), channel_id=1, source_target_pairs={{0,4},{4,8},{8,12},{12,16},{16,20},{20,24},{24,28},{28,0},{1,5},{5... | collective-permute-start | bytes 393224 | tf_op jit(solution)/shard_map/ppermute | solution.py:68
  31.7 8.1 %collective-permute-start.3 = (bf16[512,128]{1,0:T(8,128)(2,1)S(1)}, bf16[512,128]{1,0:T(8,128)(2,1)S(1)}, u32[]{:S(2)}, u32[]{:S(2)}) collective-permute-start(bf16[512,128]{1,0:T(8,128)(2,1)S(1)} %collective-permute-done.2), channel_id=1, source_target_pairs={{0,4},{4,8},{8,12},{12,16},{16,20},{20,24},{24,28},{28,0},{1,5},{5... | collective-permute-start | bytes 393224 | tf_op jit(solution)/shard_map/ppermute | solution.py:68
  39.8 7.7 %collective-permute-start.4 = (bf16[512,128]{1,0:T(8,128)(2,1)S(1)}, bf16[512,128]{1,0:T(8,128)(2,1)S(1)}, u32[]{:S(2)}, u32[]{:S(2)}) collective-permute-start(bf16[512,128]{1,0:T(8,128)(2,1)S(1)} %collective-permute-done.3), channel_id=1, source_target_pairs={{0,4},{4,8},{8,12},{12,16},{16,20},{20,24},{24,28},{28,0},{1,5},{5... | collective-permute-start | bytes 393224 | tf_op jit(solution)/shard_map/ppermute | solution.py:68
  47.5 9.5 %collective-permute-start.5 = (bf16[512,128]{1,0:T(8,128)(2,1)S(1)}, bf16[512,128]{1,0:T(8,128)(2,1)S(1)}, u32[]{:S(2)}, u32[]{:S(2)}) collective-permute-start(bf16[512,128]{1,0:T(8,128)(2,1)S(1)} %collective-permute-done.4), channel_id=1, source_target_pairs={{0,4},{4,8},{8,12},{12,16},{16,20},{20,24},{24,28},{28,0},{1,5},{5... | collective-permute-start | bytes 393224 | tf_op jit(solution)/shard_map/ppermute | solution.py:68
  56.9 7.7 %collective-permute-start.6 = (bf16[512,128]{1,0:T(8,128)(2,1)S(1)}, bf16[512,128]{1,0:T(8,128)(2,1)S(1)}, u32[]{:S(2)}, u32[]{:S(2)}) collective-permute-start(bf16[512,128]{1,0:T(8,128)(2,1)S(1)} %collective-permute-done.5), channel_id=1, source_target_pairs={{0,4},{4,8},{8,12},{12,16},{16,20},{20,24},{24,28},{28,0},{1,5},{5... | collective-permute-start | bytes 393224 | tf_op jit(solution)/shard_map/ppermute | solution.py:68
  58.7 6.1 %copy-start.5 = (bf16[512,128]{1,0:T(8,128)(2,1)S(1)}, bf16[512,128]{1,0:T(8,128)(2,1)}, u32[]{:S(2)}) copy-start(bf16[512,128]{1,0:T(8,128)(2,1)} %param.15) | copy-start | bytes 393220
  69.8 1.0 copy-start.1
  72.3 0.8 copy-start.2
  74.5 1.0 copy-start.1
  79.2 1.0 copy-start.1
  81.8 0.8 copy-start.2
  84.0 1.0 copy-start.1
  88.7 1.0 copy-start.1
  91.3 0.8 copy-start.2
  93.4 1.0 copy-start.1
  98.2 1.0 copy-start.1
  102.9 1.0 copy-start.1
  105.5 0.8 copy-start.2
  109.7 28.7 %copy-start.3 = (bf16[128,2048]{1,0:T(8,128)(2,1)S(1)}, bf16[128,2048]{1,0:T(8,128)(2,1)}, u32[]{:S(2)}) copy-start(bf16[128,2048]{1,0:T(8,128)(2,1)} %param.18) | copy-start | bytes 1572868
  109.7 30.0 %copy-start.6 = (f32[2048]{0:T(1024)S(1)}, f32[2048]{0:T(1024)}, u32[]{:S(2)}) copy-start(f32[2048]{0:T(1024)} %param.20) | copy-start | bytes 24580
  109.8 54.8 %all-gather.8.cloned.1.call-start = ((), (), s32[]{:S(2)}) async-start(), calls=%async_computation.4 | async-start | bytes 2621440 | tf_op jit(solution)/shard_map/all_gather | solution.py:141
  141.8 117.1 %all-gather.10.cloned.1.call-start = ((), (), s32[]{:S(2)}) async-start(), calls=%async_computation.5 | async-start | bytes 6488064 | tf_op jit(solution)/shard_map/all_gather | solution.py:80
  142.4 209.1 %all-gather.12.cloned.1.call-start = ((), (), s32[]{:S(2)}) async-start(), calls=%async_computation.6 | async-start | bytes 6488064 | tf_op jit(solution)/shard_map/all_gather | solution.py:81
  143.0 301.7 %all-gather.14.cloned.1.call-start = ((), (), s32[]{:S(2)}) async-start(), calls=%async_computation.7 | async-start | bytes 6488064 | tf_op jit(solution)/shard_map/all_gather | solution.py:82
  143.6 344.6 %reduce-scatter.5.cloned.1.call-start = ((), (), s32[]{:S(2)}) async-start(), calls=%async_computation.8 | async-start | bytes 2621440 | tf_op jit(solution)/shard_map/reduce_scatter | solution.py:145
  458.7 29.5 %copy-start.4 = (bf16[128,2048]{1,0:T(8,128)(2,1)S(1)}, bf16[128,2048]{1,0:T(8,128)(2,1)}, u32[]{:S(2)}) copy-start(bf16[128,2048]{1,0:T(8,128)(2,1)} %reduce-scatter.3.cloned.1.call-done) | copy-start | bytes 1572868
  (4 other events, 3.2 us)
Sparse Core Ops, SparseCore 0:
  17.7 43.8 all-gather.5
  109.9 28.5 reduce-scatter.2
  141.9 22.5 all-gather.7
  166.6 92.3 all-gather.9
  261.0 90.4 all-gather.11
  353.4 91.2 all-gather.13
  458.8 29.3 reduce-scatter.4
